TPU v7x, 256 devices: a 4x2x16 block of a 4x16x16 slice. The times are simulated.
256 devices in a mesh: grp: 2 (over y), sp: 16 (over z), dp: 8 (over x, core).
Axes of the slice: x: 4, y: 2, z: 16, core: 2. Of those that a mesh axis runs over, the one named last changes fastest.
The devices are a block of a 4x16x16 slice.
Arguments:
- activations: bfloat16 [16, 8192, 2048], P(('grp', 'dp'), 'sp'), parts along dimension 0, may hold values from -6 to 6
- value_weight: bfloat16 [2048, 1024], P('sp', 'dp'), may hold values from -0.125 to 0.125
- gate_weight: bfloat16 [2048, 1024], P('sp', 'dp'), may hold values from -0.125 to 0.125
- conv_taps: float32 [31, 1024], replicated, may hold values from -4 to 4
- conv_bias: float32 [1024], replicated, may hold values from -3 to 3
- norm_gain: float32 [1024], replicated, may hold values from 0.1 to 1.9
- norm_bias: float32 [1024], replicated, may hold values from -3 to 3
- out_weight: bfloat16 [1024, 2048], P('sp', 'dp'), may hold values from -0.1875 to 0.1875
Outputs:
- mixed_out: bfloat16 [16, 8192, 2048], P(('grp', 'dp'), 'sp'), parts along dimension 0
There are 2 independent parts, one for each index of `grp`. A program takes and returns all parts, laid end to end along the dimension named above; an argument that names none is the same for every part. Nothing has to cross between parts.
All inputs are finite; a program needn't handle non-finite values.
Results may differ from a plain program's by a relative error of at most 0.013.
Values may be sent and summed in bfloat16 or wider, within the bound.
No kernel may reach another device: no remote copies, remote signals or barrier semaphores. Data moves between devices by JAX's collectives and lax.ppermute only.
A program may use at most 64 MiB of HBM per device.

v0:
```python
import jax
import jax.numpy as jnp
from jax import lax
from jax.sharding import PartitionSpec as P

epsilon = 1e-05


def in_one_piece(arrays, axis, dim, along):
    widths = [a.shape[along] for a in arrays]
    both = jnp.concatenate(arrays, axis=along)
    filled = lax.all_gather(both, axis, axis=dim, tiled=True)
    return tuple(jnp.split(filled, [sum(widths[:k]) for k in range(1, len(widths))], axis=along))


def passed_along(value, axis, steps):
    count = lax.axis_size(axis)
    first, last = (max(0, -steps), min(count, count - steps))
    return lax.ppermute(value, axis, [(source, source + steps) for source in range(first, last)])


def local(
    activations, value_weight, gate_weight, conv_taps, conv_bias, norm_gain, norm_bias, out_weight
):
    tokens = activations[0]
    tok_rows = tokens.shape[0]
    kernel_len = conv_taps.shape[0]
    whole_value, whole_gate = in_one_piece((value_weight, gate_weight), "sp", 0, 1)
    stacked = jnp.stack([whole_value, whole_gate], axis=0)
    both_rows = jnp.einsum(
        "td,kdc->ktc",
        tokens,
        lax.all_gather(stacked, "dp", axis=2, tiled=True),
        preferred_element_type=jnp.float32,
    )
    value_rows = both_rows[0]
    gate_rows = both_rows[1]
    value_half = value_rows.astype(jnp.bfloat16)
    gate_half = gate_rows.astype(jnp.bfloat16)
    gated_rows = (
        value_half.astype(jnp.float32) * jax.nn.sigmoid(gate_half.astype(jnp.float32))
    ).astype(jnp.bfloat16)
    prior = passed_along(gated_rows[tok_rows - (kernel_len - 1) :], "sp", 1)
    padded = jnp.concatenate([prior, gated_rows], axis=0).astype(jnp.float32)
    conv_sum = jnp.zeros(gated_rows.shape, jnp.float32) + conv_bias[None, :]
    for tap_index in range(kernel_len):
        conv_sum = (
            conv_sum + conv_taps[tap_index][None, :] * padded[tap_index : tap_index + tok_rows]
        )
    mean_row = jnp.mean(conv_sum, axis=-1, keepdims=True)
    centered = conv_sum - mean_row
    spread = jnp.mean(centered * centered, axis=-1, keepdims=True)
    normed = centered * lax.rsqrt(spread + epsilon) * norm_gain[None, :] + norm_bias[None, :]
    swished = jax.nn.silu(normed).astype(jnp.bfloat16)
    whole_output = lax.all_gather(out_weight, "sp", axis=0, tiled=True)
    result = jnp.dot(
        swished,
        lax.all_gather(whole_output, "dp", axis=1, tiled=True),
        preferred_element_type=jnp.float32,
    )
    return result.astype(jnp.bfloat16)[None]


def solution(mesh):
    in_specs = (
        P(("grp", "dp"), "sp", None),
        P("sp", "dp"),
        P("sp", "dp"),
        P(),
        P(),
        P(),
        P(),
        P("sp", "dp"),
    )
    out_specs = P(("grp", "dp"), "sp", None)
    return jax.shard_map(local, mesh=mesh, in_specs=in_specs, out_specs=out_specs, check_vma=False)
```

profile of v0, /device:TPU:33, one launch (start us, length us, event | category | flops | bytes accessed | tf_op | source)
XLA Modules:
  0.0 210.3 jit_solution(13872795906434215468)
XLA Ops:
  6.5 0.0 copy-start
  6.6 0.0 all-gather.4.cloned.1.call-start
  6.6 1.6 pad_maximum_fusion.1
  8.1 0.1 all-gather.4.cloned.1.call-update
  8.2 0.1 all-gather.6.cloned.1.call-start
  8.2 73.8 %all-gather.4.cloned.1.call-done = bf16[2048,256]{1,0:T(8,128)(2,1)} async-done(((bf16[128,256]{1,0:T(8,128)(2,1)}), bf16[2048,256]{1,0:T(8,128)(2,1)}) %all-gather.4.cloned.1.call-update) | async-done | bytes 1048592 | tf_op jit(solution)/shard_map/all_gather | solution.py:12
  82.0 1.3 slice_bitcast_fusion.1
  83.3 0.0 copy-start.3
  83.3 0.0 copy-start.2
  83.3 1.1 pad_maximum_fusion
  84.4 0.1 all-gather.6.cloned.1.call-update
  84.4 0.1 all-gather.8.cloned.1.call-start
  84.5 0.0 copy-done.3
  84.5 26.9 %all_gather.14 = bf16[1024,256]{1,0:T(8,128)(2,1)} all-gather(bf16[64,256]{1,0:T(8,128)(2,1)S(1)} %copy-done.3), channel_id=1, replica_groups=mesh['grp'=2,'sp'=16,'dp'=8] {'sp'}, dimensions={0}, use_global_device_ids=true | all-gather | bytes 557056 | tf_op jit(solution)/shard_map/all_gather | solution.py:55
  111.4 0.1 all-gather.8.cloned.1.call-update
  111.5 0.0 copy-done.2
  111.5 0.1 fusion.44
  111.6 40.7 %all-gather.6.cloned.1.call-done = bf16[2,2048,1024]{2,1,0:T(8,128)(2,1)} async-done(((bf16[2,2048,128]{2,1,0:T(8,128)(2,1)}), bf16[2,2048,1024]{2,1,0:T(8,128)(2,1)}) %all-gather.6.cloned.1.call-update) | async-done | bytes 8388624 | tf_op jit(solution)/shard_map/all_gather | solution.py:33
  152.4 0.0 copy-done
  152.4 8.1 %convert_bitcast_fusion = bf16[2,512,1024]{2,1,0:T(8,128)(2,1)S(1)} fusion(bf16[2,2048,1024]{2,1,0:T(8,128)(2,1)} %all-gather.6.cloned.1.call-done, bf16[1,512,2048]{2,1,0:T(8,128)(2,1)S(1)} %copy-done), kind=kOutput, calls=%fused_computation.67 | convolution fusion | flops 4296015872 | bytes 12582912 | tf_op jit(solution)/shard_map/td,kdc->ktc/dot_general | solution.py:30
  160.4 0.6 multiply_convert_fusion
  161.1 3.2 %collective-permute-start = (bf16[30,1024]{1,0:T(8,128)(2,1)S(1)}, bf16[30,1024]{1,0:T(8,128)(2,1)S(1)}, u32[]{:S(2)}, u32[]{:S(2)}) collective-permute-start(bf16[30,1024]{1,0:T(8,128)(2,1)S(1)} %slice_bitcast_fusion.2), channel_id=1, source_target_pairs={{0,8},{8,16},{16,24},{24,32},{32,40},{40,48},{48,56},{56,64},{64,7... | collective-permute-start | bytes 184328 | tf_op jit(solution)/shard_map/ppermute | solution.py:19
  164.3 0.6 fusion.48
  164.9 0.0 copy-start.4
  164.9 0.7 collective-permute-done
  165.6 0.3 maximum_convert_fusion
  165.9 0.0 copy-done.4
  165.9 9.8 %fusion.42 = (f32[512]{0:T(512)S(1)}, f32[512,1024]{1,0:T(8,128)S(1)}) fusion(f32[542,1024]{1,0:T(8,128)S(1)} %maximum_convert_fusion, f32[1024]{0:T(1024)S(1)} %bitcast.61, f32[1024]{0:T(1024)S(1)} %bitcast.62, f32[1024]{0:T(1024)S(1)} %bitcast.64, f32[1024]{0:T(1024)S(1)} %bitcast.65, f32[1024]{0:T(1024)S(1)} %bitcast.66, f32[1024]{0:T(1024)S(1)} %bitcast.67, ...), kind=kLoop, calls=%fused_computation.84 | loop fusion | flops 33029632 | bytes 67241984 | tf_op jit(solution)/shard_map/reduce_sum | solution.py:50
  175.7 0.0 copy-start.1
  175.8 0.0 copy-start.5
  175.8 0.0 copy-start.6
  175.8 1.3 copy-done.1
  177.1 0.3 multiply_reduce_fusion
  177.4 19.4 %all-gather.8.cloned.1.call-done = bf16[1024,2048]{1,0:T(8,128)(2,1)} async-done(((bf16[1024,256]{1,0:T(8,128)(2,1)}), bf16[1024,2048]{1,0:T(8,128)(2,1)}) %all-gather.8.cloned.1.call-update) | async-done | bytes 4194320 | tf_op jit(solution)/shard_map/all_gather | solution.py:58
  196.8 0.0 copy-done.5
  196.8 0.0 copy-done.6
  196.8 7.0 %fusion = bf16[1,512,2048]{2,1,0:T(8,128)(2,1)} fusion(bf16[1024,2048]{1,0:T(8,128)(2,1)} %all-gather.8.cloned.1.call-done, f32[512,1024]{1,0:T(8,128)} %copy-done.1, f32[1024]{0:T(1024)S(1)} %copy-done.5, f32[1024]{0:T(1024)S(1)} %copy-done.6, f32[512]{0:T(512)S(1)} %add_rsqrt_fusion, f32[512]{0:T(512)S(1)} %broadcast_multiply_fusion), kind=kOutput, calls=%fused_computation.1 | convolution fusion | flops 2153250816 | bytes 8400896 | tf_op jit(solution)/shard_map/dot_general | solution.py:56
  (4 shorter events, 0.1 us)
Async XLA Ops:
  6.5 145.8 %copy-start = (bf16[1,512,2048]{2,1,0:T(8,128)(2,1)S(1)}, bf16[1,512,2048]{2,1,0:T(8,128)(2,1)}, u32[]{:S(2)}) copy-start(bf16[1,512,2048]{2,1,0:T(8,128)(2,1)} %param.8) | copy-start | bytes 6291460
  6.6 75.5 %all-gather.4.cloned.1.call-start = ((), (), s32[]{:S(2)}) async-start(), calls=%async_computation | async-start | bytes 1114112 | tf_op jit(solution)/shard_map/all_gather | solution.py:12
  8.2 144.2 %all-gather.6.cloned.1.call-start = ((), (), s32[]{:S(2)}) async-start(), calls=%async_computation.1 | async-start | bytes 9437184 | tf_op jit(solution)/shard_map/all_gather | solution.py:33
  83.3 1.2 copy-start.3
  83.3 28.2 %copy-start.2 = (f32[31,1024]{1,0:T(8,128)S(1)}, f32[31,1024]{1,0:T(8,128)}, u32[]{:S(2)}) copy-start(f32[31,1024]{1,0:T(8,128)} %param.11) | copy-start | bytes 380932
  84.4 112.4 %all-gather.8.cloned.1.call-start = ((), (), s32[]{:S(2)}) async-start(), calls=%async_computation.2 | async-start | bytes 4718592 | tf_op jit(solution)/shard_map/all_gather | solution.py:58
  161.1 4.5 %collective-permute-start = (bf16[30,1024]{1,0:T(8,128)(2,1)S(1)}, bf16[30,1024]{1,0:T(8,128)(2,1)S(1)}, u32[]{:S(2)}, u32[]{:S(2)}) collective-permute-start(bf16[30,1024]{1,0:T(8,128)(2,1)S(1)} %slice_bitcast_fusion.2), channel_id=1, source_target_pairs={{0,8},{8,16},{16,24},{24,32},{32,40},{40,48},{48,56},{56,64},{64,7... | collective-permute-start | bytes 184328 | tf_op jit(solution)/shard_map/ppermute | solution.py:19
  164.9 1.0 copy-start.4
  175.7 1.3 copy-start.1
  175.8 21.1 %copy-start.5 = (f32[1024]{0:T(1024)S(1)}, f32[1024]{0:T(1024)}, u32[]{:S(2)}) copy-start(f32[1024]{0:T(1024)} %param.14) | copy-start | bytes 12292
  175.8 21.1 %copy-start.6 = (f32[1024]{0:T(1024)S(1)}, f32[1024]{0:T(1024)}, u32[]{:S(2)}) copy-start(f32[1024]{0:T(1024)} %param.13) | copy-start | bytes 12292
Sparse Core Ops, SparseCore 0:
  9.1 72.8 all-gather.3
  84.6 67.7 all-gather.5
  154.2 42.5 all-gather.7
where the time goes:
time: 211 us; the launch traced here: 210 us
  waiting for transfers between devices  135 us (64%)
  blocking collectives  26.9 us (13%)
  matrix products  15 us (7%)
  other arithmetic  14.3 us (7%)
  between operations  13.3 us (6%)
  starting transfers between devices  3.33 us (2%)
  local copies, waits for them, and re-layouts  2.71 us (1%)
    all_gather x1, waiting for transfers between devices, in_one_piece(): filled = lax.all_gather(both, axis, axis=dim, tiled=True)  73.8 us
    all_gather x1, waiting for transfers between devices, local(): lax.all_gather(stacked, 'dp', axis=2, tiled=True)  40.7 us
    all_gather x1, blocking collectives, local(): whole_output = lax.all_gather(out_weight, 'sp', axis=0, tiled=True)  26.9 us
    all_gather x1, waiting for transfers between devices, local(): lax.all_gather(whole_output, 'dp', axis=1, tiled=True)  19.4 us
    reduce_sum x1, other arithmetic, local(): mean_row = jnp.mean(conv_sum, axis=-1, keepdims=True)  9.83 us
    dot_general x1, matrix products, local(): jnp.einsum('td,kdc->ktc', tokens, lax.all_gather(stacked, 'dp', axis=2, t...  8.07 us
    dot_general x1, matrix products, local(): jnp.dot(swished, lax.all_gather(whole_output, 'dp', axis=1, tiled=True),...  6.97 us
  transfers between devices with their start and end apart: 4, of which 4 were waited for; matrix products, arithmetic and copies ran while one was open for 9% of the time, Pallas kernels for 0%

commit v1 on v0

--- a/solution.py
+++ b/solution.py
@@ -4,6 +4,15 @@
 from jax.sharding import PartitionSpec as P
 
 epsilon = 1e-05
+case_get = lambda patch, mesh_ax: jnp.concatenate(
+    lax.all_to_all(
+        jnp.stack([patch] * lax.axis_size(mesh_ax), 0),
+        split_axis=0,
+        concat_axis=0,
+        axis_name=mesh_ax,
+    ),
+    axis=2,
+)
 
 
 def in_one_piece(arrays, axis, dim, along):
@@ -28,10 +37,7 @@
     whole_value, whole_gate = in_one_piece((value_weight, gate_weight), "sp", 0, 1)
     stacked = jnp.stack([whole_value, whole_gate], axis=0)
     both_rows = jnp.einsum(
-        "td,kdc->ktc",
-        tokens,
-        lax.all_gather(stacked, "dp", axis=2, tiled=True),
-        preferred_element_type=jnp.float32,
+        "td,kdc->ktc", tokens, case_get(stacked, "dp"), preferred_element_type=jnp.float32
     )
     value_rows = both_rows[0]
     gate_rows = both_rows[1]

time: 211 us -> 256 us (1.21)
  waiting for transfers between devices: 135 us -> 156 us
  starting transfers between devices: 3.33 us -> 19.5 us
  local copies, waits for them, and re-layouts: 2.71 us -> 7.57 us
    all_to_all x0 -> x1, waiting for transfers between devices: none -> 81.6 us  [lax.all_to_all(jnp.stack([patch] * lax.axis_size(mesh_ax), 0), split_axis...]
    all_gather x1 -> x0, waiting for transfers between devices: 40.7 us -> none  [local(): lax.all_gather(stacked, 'dp', axis=2, tiled=True)]
    all_gather x1, waiting for transfers between devices: 19.4 us -> 0.03 us  [local(): lax.all_gather(whole_output, 'dp', axis=1, tiled=True)]
    all_to_all x0 -> x1, starting transfers between devices: none -> 16.5 us  [lax.all_to_all(jnp.stack([patch] * lax.axis_size(mesh_ax), 0), split_axis...]
    another operation x0 -> x1, local copies, waits for them, and re-layouts: none -> 4.86 us  [jnp.stack([patch] * lax.axis_size(mesh_ax), 0)]
  transfers between devices with their start and end apart: 4 -> 4, of which waited for: 4 -> 3; matrix products, arithmetic and copies ran while one was open for 9% -> 8% of each run, Pallas kernels for 0% -> 0%
where the time goes in v1:
time: 256 us
  waiting for transfers between devices  156 us (61%)
  blocking collectives  28.9 us (11%)
  starting transfers between devices  19.5 us (8%)
  matrix products  15 us (6%)
  between operations  15 us (6%)
  other arithmetic  13.3 us (5%)
  local copies, waits for them, and re-layouts  7.57 us (3%)
    all_to_all x1, waiting for transfers between devices, lax.all_to_all(jnp.stack([patch] * lax.axis_size(mesh_ax), 0), split_axis...  81.6 us
    all_gather x1, waiting for transfers between devices, in_one_piece(): filled = lax.all_gather(both, axis, axis=dim, tiled=True)  73.8 us
    all_gather x1, blocking collectives, local(): whole_output = lax.all_gather(out_weight, 'sp', axis=0, tiled=True)  28.9 us
    all_to_all x1, starting transfers between devices, lax.all_to_all(jnp.stack([patch] * lax.axis_size(mesh_ax), 0), split_axis...  16.5 us
    reduce_sum x1, other arithmetic, local(): mean_row = jnp.mean(conv_sum, axis=-1, keepdims=True)  9.83 us
    dot_general x1, matrix products, local(): jnp.einsum('td,kdc->ktc', tokens, case_get(stacked, 'dp'), preferred_elem...  8.06 us
    dot_general x1, matrix products, local(): jnp.dot(swished, lax.all_gather(whole_output, 'dp', axis=1, tiled=True),...  6.97 us
  transfers between devices with their start and end apart: 4, of which 3 were waited for; matrix products, arithmetic and copies ran while one was open for 8% of the time, Pallas kernels for 0%

profile of v1, /device:TPU:33, one launch (start us, length us, event | category | flops | bytes accessed | tf_op | source)
XLA Modules:
  0.0 255.7 jit_solution(10089651937803572025)
XLA Ops:
  7.4 0.0 copy-start
  7.4 0.0 all-gather.3.cloned.1.call-start
  7.4 1.6 pad_maximum_fusion.1
  9.0 0.1 all-gather.3.cloned.1.call-update
  9.0 73.8 %all-gather.3.cloned.1.call-done = bf16[2048,256]{1,0:T(8,128)(2,1)} async-done(((bf16[128,256]{1,0:T(8,128)(2,1)}), bf16[2048,256]{1,0:T(8,128)(2,1)}) %all-gather.3.cloned.1.call-update) | async-done | bytes 1048592 | tf_op jit(solution)/shard_map/all_gather | solution.py:21
  82.9 1.3 slice_bitcast_fusion.1
  84.1 0.1 pad_maximum_fusion
  84.2 4.9 %stack.11 = bf16[8,2,2048,128]{3,2,1,0:T(8,128)(2,1)} broadcast(bf16[2,2048,128]{2,1,0:T(8,128)(2,1)S(1)} %pad_maximum_fusion), dimensions={1,2,3} | broadcast | bytes 9437184 | tf_op jit(solution)/shard_map/stack | solution.py:9
  89.1 0.0 copy-start.3
  89.1 0.0 copy-start.2
  89.1 16.5 %all-to-all-start = ((bf16[8,2,2048,128]{3,2,1,0:T(8,128)(2,1)}), bf16[8,2,2048,128]{3,2,1,0:T(8,128)(2,1)}, u32[]{:S(2)}, u32[]{:S(2)}) async-start(bf16[8,2,2048,128]{3,2,1,0:T(8,128)(2,1)} %stack.11), calls=%async_computation | async-start | bytes 16777216 | tf_op jit(solution)/shard_map/all_to_all | solution.py:8
  105.6 0.0 all-gather.5.cloned.1.call-start
  105.6 0.0 copy-done.3
  105.6 28.9 %all_gather.10 = bf16[1024,256]{1,0:T(8,128)(2,1)} all-gather(bf16[64,256]{1,0:T(8,128)(2,1)S(1)} %copy-done.3), channel_id=1, replica_groups=mesh['grp'=2,'sp'=16,'dp'=8] {'sp'}, dimensions={0}, use_global_device_ids=true | all-gather | bytes 557056 | tf_op jit(solution)/shard_map/all_gather | solution.py:61
  134.5 0.1 all-gather.5.cloned.1.call-update
  134.6 0.0 copy-done.2
  134.6 0.1 fusion.48
  134.7 81.6 %all-to-all-done = bf16[8,2,2048,128]{3,2,1,0:T(8,128)(2,1)} async-done(((bf16[8,2,2048,128]{3,2,1,0:T(8,128)(2,1)}), bf16[8,2,2048,128]{3,2,1,0:T(8,128)(2,1)}, u32[]{:S(2)}, u32[]{:S(2)}) %all-to-all-start) | async-done | bytes 8388640 | tf_op jit(solution)/shard_map/all_to_all | solution.py:8
  216.3 0.0 copy-done
  216.3 8.1 %convert_bitcast_fusion = bf16[2,512,1024]{2,1,0:T(8,128)(2,1)S(1)} fusion(bf16[1,512,2048]{2,1,0:T(8,128)(2,1)S(1)} %copy-done, bf16[8,2,2048,128]{3,2,1,0:T(8,128)(2,1)} %all-to-all-done), kind=kOutput, calls=%fused_computation.69 | convolution fusion | flops 4296015872 | bytes 12582912 | tf_op jit(solution)/shard_map/td,kdc->ktc/dot_general | solution.py:39
  224.4 0.6 multiply_convert_fusion
  225.0 3.1 %collective-permute-start = (bf16[30,1024]{1,0:T(8,128)(2,1)S(1)}, bf16[30,1024]{1,0:T(8,128)(2,1)S(1)}, u32[]{:S(2)}, u32[]{:S(2)}) collective-permute-start(bf16[30,1024]{1,0:T(8,128)(2,1)S(1)} %slice_bitcast_fusion.2), channel_id=1, source_target_pairs={{0,8},{8,16},{16,24},{24,32},{32,40},{40,48},{48,56},{56,64},{64,7... | collective-permute-start | bytes 184328 | tf_op jit(solution)/shard_map/ppermute | solution.py:28
  228.1 0.6 fusion.51
  228.7 0.0 copy-start.4
  228.7 0.7 collective-permute-done
  229.4 0.3 maximum_convert_fusion
  229.7 0.0 copy-done.4
  229.7 9.8 %fusion.46 = (f32[512]{0:T(512)S(1)}, f32[512,1024]{1,0:T(8,128)S(1)}) fusion(f32[542,1024]{1,0:T(8,128)S(1)} %maximum_convert_fusion, f32[1024]{0:T(1024)S(1)} %bitcast.70, f32[1024]{0:T(1024)S(1)} %bitcast.71, f32[1024]{0:T(1024)S(1)} %bitcast.73, f32[1024]{0:T(1024)S(1)} %bitcast.74, f32[1024]{0:T(1024)S(1)} %bitcast.75, f32[1024]{0:T(1024)S(1)} %bitcast.76, ...), kind=kLoop, calls=%fused_computation.86 | loop fusion | flops 33029632 | bytes 67241984 | tf_op jit(solution)/shard_map/reduce_sum | solution.py:56
  239.5 0.0 copy-start.1
  239.5 0.0 copy-start.5
  239.5 0.0 copy-start.6
  239.6 1.3 copy-done.1
  240.9 0.3 multiply_reduce_fusion
  241.2 0.0 all-gather.5.cloned.1.call-done
  241.2 0.0 copy-done.5
  241.3 0.0 copy-done.6
  241.3 7.0 %fusion.3 = bf16[1,512,2048]{2,1,0:T(8,128)(2,1)} fusion(bf16[1024,2048]{1,0:T(8,128)(2,1)} %all-gather.5.cloned.1.call-done, f32[512,1024]{1,0:T(8,128)} %copy-done.1, f32[1024]{0:T(1024)S(1)} %copy-done.5, f32[1024]{0:T(1024)S(1)} %copy-done.6, f32[512]{0:T(512)S(1)} %add_rsqrt_fusion, f32[512]{0:T(512)S(1)} %broadcast_multiply_fusion), kind=kOutput, calls=%fused_computation.4 | convolution fusion | flops 2153250816 | bytes 8400896 | tf_op jit(solution)/shard_map/dot_general | solution.py:62
  (4 shorter events, 0.1 us)
Async XLA Ops:
  7.4 208.9 %copy-start = (bf16[1,512,2048]{2,1,0:T(8,128)(2,1)S(1)}, bf16[1,512,2048]{2,1,0:T(8,128)(2,1)}, u32[]{:S(2)}) copy-start(bf16[1,512,2048]{2,1,0:T(8,128)(2,1)} %param.8) | copy-start | bytes 6291460
  7.4 75.5 %all-gather.3.cloned.1.call-start = ((), (), s32[]{:S(2)}) async-start(), calls=%async_computation.1 | async-start | bytes 1114112 | tf_op jit(solution)/shard_map/all_gather | solution.py:21
  89.1 16.5 %copy-start.3 = (bf16[64,256]{1,0:T(8,128)(2,1)S(1)}, bf16[64,256]{1,0:T(8,128)(2,1)}, u32[]{:S(2)}) copy-start(bf16[64,256]{1,0:T(8,128)(2,1)} %param.15) | copy-start | bytes 98308
  89.1 45.5 %copy-start.2 = (f32[31,1024]{1,0:T(8,128)S(1)}, f32[31,1024]{1,0:T(8,128)}, u32[]{:S(2)}) copy-start(f32[31,1024]{1,0:T(8,128)} %param.11) | copy-start | bytes 380932
  89.1 127.2 %all-to-all-start = ((bf16[8,2,2048,128]{3,2,1,0:T(8,128)(2,1)}), bf16[8,2,2048,128]{3,2,1,0:T(8,128)(2,1)}, u32[]{:S(2)}, u32[]{:S(2)}) async-start(bf16[8,2,2048,128]{3,2,1,0:T(8,128)(2,1)} %stack.11), calls=%async_computation | async-start | bytes 16777216 | tf_op jit(solution)/shard_map/all_to_all | solution.py:8
  105.6 135.7 %all-gather.5.cloned.1.call-start = ((), (), s32[]{:S(2)}) async-start(), calls=%async_computation.2 | async-start | bytes 4718592 | tf_op jit(solution)/shard_map/all_gather | solution.py:64
  225.0 4.4 %collective-permute-start = (bf16[30,1024]{1,0:T(8,128)(2,1)S(1)}, bf16[30,1024]{1,0:T(8,128)(2,1)S(1)}, u32[]{:S(2)}, u32[]{:S(2)}) collective-permute-start(bf16[30,1024]{1,0:T(8,128)(2,1)S(1)} %slice_bitcast_fusion.2), channel_id=1, source_target_pairs={{0,8},{8,16},{16,24},{24,32},{32,40},{40,48},{48,56},{56,64},{64,7... | collective-permute-start | bytes 184328 | tf_op jit(solution)/shard_map/ppermute | solution.py:28
  228.7 1.0 copy-start.4
  239.5 1.3 copy-start.1
  239.5 1.7 copy-start.5
  239.5 1.7 copy-start.6
Sparse Core Ops, SparseCore 0:
  10.0 72.8 all-gather.2
Sparse Core Ops, SparseCore 1:
  134.6 68.1 all-gather.4
